TPU v7x, 32 devices: a whole 2x2x4 slice. The times are simulated.
32 devices in a mesh: sp: 8 (over z, core), tp: 4 (over y, x).
Axes of the slice: x: 2, y: 2, z: 4, core: 2. Of those that a mesh axis runs over, the one named last changes fastest.
Arguments:
- queries: bfloat16 [4096, 1024], P('sp', 'tp'), may hold values from -20 to 20
- key_vectors: bfloat16 [4096, 1024], P('sp', 'tp'), may hold values from -20 to 20
- value_vectors: bfloat16 [4096, 1024], P('sp', 'tp'), may hold values from -6 to 6
- log_gate_sums: float32 [4096, 16], P('sp', 'tp'), may hold values from -588 to 0, as said below
- residual: bfloat16 [4096, 2048], P('sp', 'tp'), may hold values from -24 to 24
- out_weight: bfloat16 [1024, 2048], P(None, 'tp'), may hold values from -0.75 to 0.75
- norm_gain: bfloat16 [2048], replicated, may hold values from 0.099609375 to 1.8984375
- routes: int32 [4096, 2], P('sp'), may hold values from 0 to 31, all different within a row; in each aligned block of 512 rows (0 to 511, 512 to 1023, ...) at most 40 rows name the same one
- route_weight: float32 [4096, 2], P('sp'), may hold values from 0.5 to 1.5
- expert_gate: bfloat16 [32, 2048, 512], P('sp', None, 'tp'), may hold values from -0.125 to 0.125
- expert_up: bfloat16 [32, 2048, 512], P('sp', None, 'tp'), may hold values from -0.125 to 0.125
- expert_down: bfloat16 [32, 512, 2048], P('sp', None, 'tp'), may hold values from -0.25 to 0.25
- shared_gate: bfloat16 [2048, 512], P(None, 'tp'), may hold values from -0.125 to 0.125
- shared_up: bfloat16 [2048, 512], P(None, 'tp'), may hold values from -0.125 to 0.125
- shared_down: bfloat16 [512, 2048], P(None, 'tp'), may hold values from -0.25 to 0.25
Outputs:
- layer_out: bfloat16 [4096, 2048], P('sp', 'tp')
Inputs may be any that keep to these rules, and one draw needn't show every extreme that they name: `log_gate_sums`: for each head the values do not rise along the positions. `routes`: each row names 2 different experts; among the rows of one index of sp no expert is named by more than 40 rows, a bound that some block reaches.
All inputs are finite; a program needn't handle non-finite values.
Results may differ from a plain program's by a relative error of at most 0.014.
Values may be sent and summed in bfloat16 or wider, within the bound.
A program may use at most 64 MiB of HBM per device.

v0:
```python
import math
import jax
import jax.numpy as jnp
from jax import lax
from jax.sharding import PartitionSpec as P

HDIM = 64
EPSILON = 1e-06


def silu_gate(gate_part, up_part):
    return jax.nn.silu(gate_part) * up_part


def slot_targets(routes, experts_all, capacity):
    flat_routes = routes.reshape(-1)
    onehot = (flat_routes[:, None] == jnp.arange(experts_all, dtype=jnp.int32)[None, :]).astype(
        jnp.int32
    )
    before = jnp.cumsum(onehot, axis=0) - onehot
    return flat_routes * capacity + jnp.sum(before * onehot, axis=1)


def keep_state(fold_state):
    return fold_state


def shards(
    queries,
    key_vectors,
    value_vectors,
    log_gate_sums,
    residual,
    out_weight,
    norm_gain,
    routes,
    route_weight,
    expert_gate,
    expert_up,
    expert_down,
    shared_gate,
    shared_up,
    shared_down,
):
    tok_dev = queries.shape[0]
    head_dim = HDIM
    local_heads = log_gate_sums.shape[1]
    local_width = residual.shape[1]
    model_width = norm_gain.shape[0]
    score_scale = head_dim ** (-0.5)
    seq_first = lax.axis_index("sp") * tok_dev
    query_heads = queries.reshape(tok_dev, local_heads, head_dim)
    query_pos = seq_first + jnp.arange(tok_dev, dtype=jnp.int32)
    own_gates = log_gate_sums.T
    all_gates = lax.all_gather(log_gate_sums, "sp", axis=0, tiled=True)
    initial = (
        jnp.full((local_heads, tok_dev), -1e30, jnp.float32),
        jnp.zeros((local_heads, tok_dev), jnp.float32),
        jnp.zeros((local_heads, tok_dev, head_dim), jnp.float32),
    )
    key_heads = key_vectors.reshape(tok_dev, local_heads, head_dim)
    value_heads = value_vectors.reshape(tok_dev, local_heads, head_dim)
    key_part = lax.all_gather(key_heads, "sp", axis=0, tiled=True)
    value_part = lax.all_gather(value_heads, "sp", axis=0, tiled=True)
    part_rows = key_part.shape[0]
    block_size = math.gcd(part_rows, 512)
    key_blocks = key_part.reshape(part_rows // block_size, block_size, local_heads, head_dim)
    value_blocks = value_part.reshape(part_rows // block_size, block_size, local_heads, head_dim)

    def one_block(fold_state, inputs):
        key_block, value_block, block_number = inputs
        block_first = block_number * block_size

        def compute(old_state):
            running_max, weight_total, summed = old_state
            gate_block = lax.dynamic_slice_in_dim(all_gates, block_first, block_size, 0).T
            scores = (
                jnp.einsum(
                    "qhd,khd->hqk", query_heads, key_block, preferred_element_type=jnp.float32
                )
                * score_scale
            )
            scores = scores + own_gates[:, :, None] - gate_block[:, None, :]
            key_pos = block_first + jnp.arange(block_size, dtype=jnp.int32)
            allowed = (key_pos[None, :] <= query_pos[:, None])[None]
            newmax = jnp.maximum(running_max, jnp.max(jnp.where(allowed, scores, -jnp.inf), axis=2))
            factor = jnp.exp(running_max - newmax)
            weight = jnp.where(allowed, jnp.exp(scores - newmax[:, :, None]), 0.0)
            weight_total = weight_total * factor + jnp.sum(weight, axis=2)
            summed = summed * factor[:, :, None] + jnp.einsum(
                "hqk,khd->hqd",
                weight.astype(jnp.bfloat16),
                value_block,
                preferred_element_type=jnp.float32,
            )
            return (newmax, weight_total, summed)

        useful = block_first <= seq_first + tok_dev - 1
        return (lax.cond(useful, compute, keep_state, fold_state), None)

    numbers = jnp.arange(part_rows // block_size, dtype=jnp.int32)
    result_state, _ = lax.scan(one_block, initial, (key_blocks, value_blocks, numbers))
    running_max, weight_total, summed = result_state
    attended = (summed / weight_total[:, :, None]).astype(jnp.bfloat16)
    attended = attended.transpose(1, 0, 2).reshape(tok_dev, local_heads * head_dim)
    weight_rows = out_weight
    projected = jnp.dot(
        lax.all_gather(attended, "tp", axis=1, tiled=True),
        weight_rows,
        preferred_element_type=jnp.float32,
    )
    mid = (residual.astype(jnp.float32) + projected).astype(jnp.bfloat16)
    mid_wide = mid.astype(jnp.float32)
    feature_first = lax.axis_index("tp") * local_width
    squares = lax.psum(jnp.sum(mid_wide * mid_wide, axis=1), "tp")
    inverse = lax.rsqrt(squares / model_width + EPSILON)
    own_gain = lax.dynamic_slice_in_dim(norm_gain, feature_first, local_width, 0).astype(
        jnp.float32
    )
    normed_own = (mid_wide * inverse[:, None] * own_gain[None, :]).astype(jnp.bfloat16)
    normed = lax.all_gather(normed_own, "tp", axis=1, tiled=True)
    shared_mid = silu_gate(
        jnp.dot(normed, shared_gate, preferred_element_type=jnp.float32),
        jnp.dot(normed, shared_up, preferred_element_type=jnp.float32),
    ).astype(jnp.bfloat16)
    weight_rows = shared_down
    shared_out = jnp.dot(
        lax.all_gather(shared_mid, "tp", axis=1, tiled=True),
        weight_rows,
        preferred_element_type=jnp.float32,
    )
    exp_dev = expert_gate.shape[0]
    sp_count = lax.axis_size("sp")
    experts_all = exp_dev * sp_count
    top_count = routes.shape[1]
    capacity = 5 * tok_dev * top_count // (4 * experts_all)
    targets = slot_targets(routes, experts_all, capacity)
    owners = (
        jnp.full((experts_all * capacity,), tok_dev, jnp.int32)
        .at[targets]
        .set(jnp.arange(tok_dev * top_count, dtype=jnp.int32) // top_count)
    )
    padded = jnp.concatenate(
        [normed_own, jnp.zeros((1, normed_own.shape[1]), jnp.bfloat16)], axis=0
    )
    outgoing = padded[owners].reshape(sp_count, exp_dev, capacity, normed_own.shape[1])
    rows_all = lax.all_gather(
        lax.all_to_all(outgoing, "sp", split_axis=0, concat_axis=0, tiled=True),
        "tp",
        axis=3,
        tiled=True,
    )
    gate_part = jnp.einsum(
        "secd,edf->secf", rows_all, expert_gate, preferred_element_type=jnp.float32
    )
    up_part = jnp.einsum("secd,edf->secf", rows_all, expert_up, preferred_element_type=jnp.float32)
    hidden = silu_gate(gate_part, up_part).astype(jnp.bfloat16)
    hidden_all = lax.all_gather(hidden, "tp", axis=3, tiled=True)
    produced = jnp.einsum(
        "secf,efd->secd", hidden_all, expert_down, preferred_element_type=jnp.float32
    ).astype(jnp.bfloat16)
    returned = lax.all_to_all(produced, "sp", split_axis=0, concat_axis=0, tiled=True)
    returned_flat = returned.reshape(experts_all * capacity, local_width)
    picked = returned_flat[targets].astype(jnp.float32).reshape(tok_dev, top_count, local_width)
    routed = jnp.sum(picked * route_weight[:, :, None], axis=1)
    return (mid_wide + shared_out + routed).astype(jnp.bfloat16)


def solution(mesh):
    placed = (
        P("sp", "tp"),
        P("sp", "tp"),
        P("sp", "tp"),
        P("sp", "tp"),
        P("sp", "tp"),
        P(None, "tp"),
        P(),
        P("sp", None),
        P("sp", None),
        P("sp", None, "tp"),
        P("sp", None, "tp"),
        P("sp", None, "tp"),
        P(None, "tp"),
        P(None, "tp"),
        P(None, "tp"),
    )
    return jax.shard_map(
        shards, mesh=mesh, in_specs=placed, out_specs=P("sp", "tp"), check_vma=False
    )
```

profile of v0, /device:TPU:0, one launch (start us, length us, event | category | flops | bytes accessed | tf_op | source)
XLA Modules:
  0.0 383.8 jit_solution(4985606902853403032)
XLA Ops:
  6.5 1.9 copy.36
  8.5 0.0 all-gather.7.cloned.1.call-start
  8.6 1.8 copy.34
  10.4 0.8 copy.40
  11.3 0.2 eq.29
  11.4 0.2 eq.25
  11.6 0.1 copy.35
  11.8 15.9 %all_gather.25 = f32[4096,4]{0,1:T(4,128)S(1)} all-gather(f32[512,4]{0,1:T(4,128)S(1)} %copy-done.9), channel_id=1, replica_groups=mesh['sp'=8,'tp'=4] {'sp'}, dimensions={0}, use_global_device_ids=true | all-gather | bytes 73728 | tf_op jit(solution)/shard_map/all_gather | solution.py:55
  27.7 13.3 %all-gather.9.cloned.1.call-done = bf16[4096,4,64]{0,2,1:T(8,128)(2,1)} async-done(((bf16[512,4,64]{0,2,1:T(8,128)(2,1)}), bf16[4096,4,64]{0,2,1:T(8,128)(2,1)}) %all-gather.9.cloned.1.call-update) | async-done | bytes 2097168 | tf_op jit(solution)/shard_map/all_gather | solution.py:64
  41.0 3.2 copy.57
  44.2 27.0 %all-gather.7.cloned.1.call-done = bf16[4096,4,64]{0,2,1:T(8,128)(2,1)} async-done(((bf16[512,4,64]{0,2,1:T(8,128)(2,1)}), bf16[4096,4,64]{0,2,1:T(8,128)(2,1)}) %all-gather.7.cloned.1.call-update) | async-done | bytes 2097168 | tf_op jit(solution)/shard_map/all_gather | solution.py:63
  71.3 3.2 copy.58
  74.6 16.6 %while.17 = (s32[]{:T(128)}, f32[4,512]{1,0:T(4,128)S(1)}, f32[4,512]{1,0:T(4,128)S(1)}, f32[4,512,64]{1,2,0:T(8,128)S(1)}, s32[8]{0:T(128)S(1)}, /*index=5*/s32...) while((s32[]{:T(128)}, f32[4,512]{1,0:T(4,128)S(1)}, ...), condition=%wide.region_5.6_spmd.clone, body=%wide.region_0.5_spmd.clone.sunk | while | flops 286790656 | bytes 15676785 | solution.py:102
  74.6 0.6 dynamic_slice.48
  75.8 6.3 %conditional.3 = ((f32[4,512]{1,0:T(4,128)S(1)}, f32[4,512]{1,0:T(4,128)S(1)}, f32[4,512,64]{1,2,0:T(8,128)S(1)})) conditional(s32[]{:T(128)} %convert_element_type.105, (f32[4,512]{1,0:T(4,128)S(1)}, f32[4,512]{1,0:T(4,128)S(1)}, f32[4,512,64]{1,2,0:T(8,128)S(1)}) %tuple.50, (s32[]{:T(128)}, s32[]{:T(128)}, bf16[8,512,4,64]{1,3,2,0:T(8,128)(2,1)}, ...), branch_computations={%region_1.1_spmd, %region_2.4_spmd} | conditional | flops 286790656 | bytes 15674446 | solution.py:99
  75.9 0.1 dynamic-slice_bitcast_fusion
  75.9 0.2 broadcast_compare_fusion
  76.2 2.2 fusion.2
  78.4 1.4 fusion.6
  79.8 2.3 fusion.10
  82.2 0.6 dynamic_slice.48
  83.5 0.6 dynamic_slice.48
  84.7 0.6 dynamic_slice.48
  86.0 0.6 dynamic_slice.48
  87.3 0.6 dynamic_slice.48
  88.6 0.6 dynamic_slice.48
  89.9 0.6 dynamic_slice.48
  91.2 0.7 divide_convert_fusion
  92.0 0.0 all-gather.15.cloned.1.call-start
  92.0 9.0 %reduce-window.6 = s32[32,8,128]{2,1,0:T(8,128)S(1)} reduce-window(s32[32,8,128]{2,1,0:T(8,128)S(1)} %fusion.56, s32[]{:T(128)} %constant.93.clone.1), window={size=1x1x128 pad=0_0x0_0x127_0}, to_apply=%region_8.9 | reduce-window | flops 4161536 | bytes 262148 | tf_op jit(solution)/shard_map/reduce-window
  101.0 0.1 slice.12
  101.1 0.1 copy.42
  101.3 0.1 copy.43
  101.4 0.1 copy.39
  101.6 0.2 mul.108
  101.8 0.1 broadcast_add_fusion.1
  101.9 4.3 %scatter_custom_fusion = s32[1280]{0:T(1024)S(1)} fusion(s32[1024]{0:T(1024)S(1)} %bitcast.129, s32[1024]{0:T(1024)S(1)} %add_select_fusion, s32[]{:T(128)} %constant.98.clone.1), kind=kCustom, calls=%fused_computation.75 | custom fusion | bytes 5124 | tf_op jit(solution)/shard_map/scatter | solution.py:141
  106.2 0.8 dynamic-slice_convert_fusion
  107.0 54.9 %all-gather.11.cloned.1.call-done = bf16[512,1024]{0,1:T(8,128)(2,1)} async-done(((bf16[512,256]{0,1:T(8,128)(2,1)}), bf16[512,1024]{0,1:T(8,128)(2,1)}) %all-gather.11.cloned.1.call-update) | async-done | bytes 1048592 | tf_op jit(solution)/shard_map/all_gather | solution.py:108
  161.9 2.5 fusion.50
  164.4 8.9 %psum.7 = f32[512]{0:T(512)S(1)} all-reduce(f32[512]{0:T(512)S(1)} %get-tuple-element.335), channel_id=1, replica_groups=mesh['sp'=8,'tp'=4] {'tp'}, use_global_device_ids=true, to_apply=%region_7.8 | all-reduce | flops 512 | bytes 4096 | tf_op jit(solution)/shard_map/psum | solution.py:115
  173.4 0.2 fusion.52
  173.6 4.7 %gather_fusion = bf16[1280,512]{1,0:T(8,128)(2,1)} fusion(bf16[513,512]{1,0:T(8,128)(2,1)S(1)} %concatenate.3, s32[2048]{0:T(1024)S(1)} %pad_clamp_fusion), kind=kCustom, calls=%fused_computation | custom fusion | bytes 2626560 | tf_op jit(solution)/shard_map/gather | solution.py:146
  178.4 36.8 %all_to_all.10 = bf16[8,4,40,512]{3,2,1,0:T(8,128)(2,1)S(1)} all-to-all(bf16[8,4,40,512]{3,2,1,0:T(8,128)(2,1)} %bitcast.116), channel_id=1, replica_groups=mesh['sp'=8,'tp'=4] {'sp'}, dimensions={0} | all-to-all | bytes 2621440 | tf_op jit(solution)/shard_map/all_to_all | solution.py:148
  215.2 1.2 copy.44
  216.4 0.2 all-gather.17.cloned.1.call-start
  216.6 59.0 %all-gather.15.cloned.1.call-done = bf16[8,4,40,2048]{3,2,0,1:T(8,128)(2,1)} async-done(((bf16[8,4,40,512]{3,2,0,1:T(8,128)(2,1)}), bf16[8,4,40,2048]{3,2,0,1:T(8,128)(2,1)}) %all-gather.15.cloned.1.call-update) | async-done | bytes 5242896 | tf_op jit(solution)/shard_map/all_gather | solution.py:147
  275.7 4.8 %fusion.37 = f32[8,4,40,128]{3,2,0,1:T(8,128)S(1)} fusion(bf16[8,4,40,2048]{3,2,0,1:T(8,128)(2,1)} %all-gather.15.cloned.1.call-done, bf16[4,2048,128]{2,1,0:T(8,128)(2,1)} %param.28), kind=kOutput, calls=%fused_computation.48 | convolution fusion | flops 671088640 | bytes 7995392 | tf_op jit(solution)/shard_map/secd,edf->secf/dot_general | solution.py:153
  280.5 0.5 copy-done.13
  281.0 2.3 fusion.46
  283.3 0.5 all-gather.13.cloned.1.call-update
  283.9 28.1 %all-gather.17.cloned.1.call-done = bf16[8,4,40,512]{3,2,0,1:T(8,128)(2,1)} async-done(((bf16[8,4,40,128]{3,2,0,1:T(8,128)(2,1)}), bf16[8,4,40,512]{3,2,0,1:T(8,128)(2,1)}) %all-gather.17.cloned.1.call-update) | async-done | bytes 1310736 | tf_op jit(solution)/shard_map/all_gather | solution.py:158
  312.0 2.2 fusion.31
  314.2 1.2 copy.45
  315.3 4.6 %all-to-all-start.1 = ((bf16[8,4,40,512]{3,2,1,0:T(8,128)(2,1)}), bf16[8,4,40,512]{3,2,1,0:T(8,128)(2,1)S(1)}, u32[]{:S(2)}, u32[]{:S(2)}) async-start(bf16[8,4,40,512]{3,2,1,0:T(8,128)(2,1)} %copy.45), calls=%async_computation.1 | async-start | bytes 2621440 | tf_op jit(solution)/shard_map/all_to_all | solution.py:162
  320.0 0.9 copy.46
  320.8 27.9 %all-gather.13.cloned.1.call-done = bf16[512,2048]{1,0:T(8,128)(2,1)} async-done(((bf16[512,512]{1,0:T(8,128)(2,1)}), bf16[512,2048]{1,0:T(8,128)(2,1)}) %all-gather.13.cloned.1.call-update) | async-done | bytes 2097168 | tf_op jit(solution)/shard_map/all_gather | solution.py:121
  348.7 2.5 fusion.62
  351.3 0.7 fusion.49
  352.0 10.6 %all_gather.29 = bf16[512,512]{1,0:T(8,128)(2,1)} all-gather(bf16[512,128]{1,0:T(8,128)(2,1)S(1)} %fusion.49), channel_id=1, replica_groups=mesh['sp'=8,'tp'=4] {'tp'}, dimensions={1}, use_global_device_ids=true | all-gather | bytes 655360 | tf_op jit(solution)/shard_map/all_gather | solution.py:128
  362.6 5.1 %gather_fusion.1 = bf16[1024,512]{1,0:T(8,128)(2,1)} fusion(bf16[1280,512]{1,0:T(8,128)(2,1)S(1)} %bitcast.115, s32[1024]{0:T(1024)S(1)} %broadcast_clamp_fusion), kind=kCustom, calls=%fused_computation.1 | custom fusion | bytes 2101248 | tf_op jit(solution)/shard_map/gather | solution.py:164
  367.7 3.4 reshape.124
  371.1 4.5 %multiply_reduce_fusion = f32[512,512]{1,0:T(8,128)S(1)} fusion(f32[512,2,512]{2,1,0:T(2,128)} %reshape.124, f32[512,2]{1,0:T(8,128)S(1)} %copy-done.7), kind=kLoop, calls=%fused_computation.38 | loop fusion | flops 786432 | bytes 3149824 | tf_op jit(solution)/shard_map/reduce_sum | solution.py:165
  375.7 1.2 fusion.36
  (73 shorter events, 0.6 us)
Async XLA Ops:
  6.5 305.4 %copy-start = (bf16[4,512,512]{2,1,0:T(8,128)(2,1)S(1)}, bf16[4,512,512]{2,1,0:T(8,128)(2,1)}, u32[]{:S(2)}) copy-start(bf16[4,512,512]{2,1,0:T(8,128)(2,1)} %param.30) | copy-start | bytes 6291460
  6.5 5.1 %copy-start.10 = (bf16[512,256]{1,0:T(8,128)(2,1)S(1)}, bf16[512,256]{1,0:T(8,128)(2,1)}, u32[]{:S(2)}) copy-start(bf16[512,256]{1,0:T(8,128)(2,1)} %param.19) | copy-start | bytes 786436
  6.5 5.2 %copy-start.9 = (f32[512,4]{0,1:T(4,128)S(1)}, f32[512,4]{0,1:T(4,128)}, u32[]{:S(2)}) copy-start(f32[512,4]{0,1:T(4,128)} %param.22) | copy-start | bytes 24580
  6.5 34.5 %all-gather.9.cloned.1.call-start = ((), (), s32[]{:S(2)}) async-start(), calls=%async_computation.3 | async-start | bytes 2359296 | tf_op jit(solution)/shard_map/all_gather | solution.py:64
  8.5 62.8 %all-gather.7.cloned.1.call-start = ((), (), s32[]{:S(2)}) async-start(), calls=%async_computation.2 | async-start | bytes 2359296 | tf_op jit(solution)/shard_map/all_gather | solution.py:63
  10.4 151.5 %all-gather.11.cloned.1.call-start = ((), (), s32[]{:S(2)}) async-start(), calls=%async_computation.4 | async-start | bytes 1310720 | tf_op jit(solution)/shard_map/all_gather | solution.py:108
  74.6 26.8 %copy-start.11 = (s32[512,2]{0,1:T(2,128)S(1)}, s32[512,2]{0,1:T(2,128)}, u32[]{:S(2)}) copy-start(s32[512,2]{0,1:T(2,128)} %param.26) | copy-start | bytes 12292
  92.0 183.7 %all-gather.15.cloned.1.call-start = ((), (), s32[]{:S(2)}) async-start(), calls=%async_computation.6 | async-start | bytes 6553600 | tf_op jit(solution)/shard_map/all_gather | solution.py:147
  164.4 9.2 %copy-start.5 = (bf16[512,512]{1,0:T(8,128)(2,1)}, bf16[512,512]{1,0:T(8,128)(2,1)S(1)}, u32[]{:S(2)}) copy-start(bf16[512,512]{1,0:T(8,128)(2,1)S(1)} %get-tuple-element.336) | copy-start | bytes 1572868
  173.6 4.8 %copy-start.2 = (bf16[512,512]{1,0:T(8,128)(2,1)}, bf16[512,512]{1,0:T(8,128)(2,1)S(1)}, u32[]{:S(2)}) copy-start(bf16[512,512]{1,0:T(8,128)(2,1)S(1)} %fusion.52) | copy-start | bytes 1572868
  216.4 95.6 %all-gather.17.cloned.1.call-start = ((), (), s32[]{:S(2)}) async-start(), calls=%async_computation.7 | async-start | bytes 1638400 | tf_op jit(solution)/shard_map/all_gather | solution.py:158
  275.7 4.8 %copy-start.1 = (bf16[8,4,40,2048]{3,2,0,1:T(8,128)(2,1)S(1)}, bf16[8,4,40,2048]{3,2,0,1:T(8,128)(2,1)}, u32[]{:S(2)}) copy-start(bf16[8,4,40,2048]{3,2,0,1:T(8,128)(2,1)} %all-gather.15.cloned.1.call-done) | copy-start | bytes 15728644
  275.7 5.3 %copy-start.13 = (bf16[4,2048,128]{2,1,0:T(8,128)(2,1)S(1)}, bf16[4,2048,128]{2,1,0:T(8,128)(2,1)}, u32[]{:S(2)}) copy-start(bf16[4,2048,128]{2,1,0:T(8,128)(2,1)} %param.29) | copy-start | bytes 6291460
  283.3 65.4 %all-gather.13.cloned.1.call-start = ((), (), s32[]{:S(2)}) async-start(), calls=%async_computation.5 | async-start | bytes 2621440 | tf_op jit(solution)/shard_map/all_gather | solution.py:121
  314.1 5.8 %copy-start.12 = (f32[512,2]{0,1:T(2,128)S(1)}, f32[512,2]{0,1:T(2,128)}, u32[]{:S(2)}) copy-start(f32[512,2]{0,1:T(2,128)} %param.27) | copy-start | bytes 12292
  315.3 47.3 %all-to-all-start.1 = ((bf16[8,4,40,512]{3,2,1,0:T(8,128)(2,1)}), bf16[8,4,40,512]{3,2,1,0:T(8,128)(2,1)S(1)}, u32[]{:S(2)}, u32[]{:S(2)}) async-start(bf16[8,4,40,512]{3,2,1,0:T(8,128)(2,1)} %copy.45), calls=%async_computation.1 | async-start | bytes 2621440 | tf_op jit(solution)/shard_map/all_to_all | solution.py:162
  348.7 2.5 copy-start.3
  348.7 2.5 copy-start.14
  367.7 3.4 copy-start.7
  371.1 4.5 %copy-start.4 = (bf16[512,512]{1,0:T(8,128)(2,1)S(1)}, bf16[512,512]{1,0:T(8,128)(2,1)}, u32[]{:S(2)}) copy-start(bf16[512,512]{1,0:T(8,128)(2,1)} %all_gather.29) | copy-start | bytes 1572868
  371.1 4.5 %copy-start.6 = (bf16[512,512]{1,0:T(8,128)(2,1)S(1)}, bf16[512,512]{1,0:T(8,128)(2,1)}, u32[]{:S(2)}) copy-start(bf16[512,512]{1,0:T(8,128)(2,1)} %copy-done.5) | copy-start | bytes 1572868
  371.1 4.6 %copy-start.8 = (bf16[512,512]{1,0:T(8,128)(2,1)S(1)}, bf16[512,512]{1,0:T(8,128)(2,1)}, u32[]{:S(2)}) copy-start(bf16[512,512]{1,0:T(8,128)(2,1)} %param.33) | copy-start | bytes 1572868
Sparse Core Ops, SparseCore 0:
  8.9 32.0 all-gather.8
  42.6 28.6 all-gather.6
  92.1 69.7 all-gather.10
  216.5 59.1 all-gather.14
  283.4 28.5 all-gather.16
  313.6 35.0 all-gather.12
where the time goes:
time: 385 us; the launch traced here: 384 us
  waiting for transfers between devices  211 us (55%)
  blocking collectives  72.3 us (19%)
  local copies, waits for them, and re-layouts  38.3 us (10%)
  matrix products  20.8 us (5%)
  other arithmetic  17.1 us (4%)
  between operations  13.8 us (4%)
  loops' own time  5.65 us (1%)
  starting transfers between devices  4.99 us (1%)
    all_gather x1, waiting for transfers between devices, shards(): lax.all_gather(lax.all_to_all(outgoing, 'sp', split_axis=0, concat_axis=0...  59 us
    all_gather x1, waiting for transfers between devices, shards(): lax.all_gather(attended, 'tp', axis=1, tiled=True)  54.9 us
    all_to_all x1, blocking collectives, shards(): lax.all_to_all(outgoing, 'sp', split_axis=0, concat_axis=0, tiled=True)  36.8 us
    all_gather x1, waiting for transfers between devices, shards(): hidden_all = lax.all_gather(hidden, 'tp', axis=3, tiled=True)  28.1 us
    all_gather x1, waiting for transfers between devices, shards(): normed = lax.all_gather(normed_own, 'tp', axis=1, tiled=True)  27.9 us
    all_gather x1, waiting for transfers between devices, shards(): key_part = lax.all_gather(key_heads, 'sp', axis=0, tiled=True)  27 us
    all_gather x1, blocking collectives, shards(): all_gates = lax.all_gather(log_gate_sums, 'sp', axis=0, tiled=True)  15.9 us
    all_gather x1, waiting for transfers between devices, shards(): value_part = lax.all_gather(value_heads, 'sp', axis=0, tiled=True)  13.3 us
  transfers between devices with their start and end apart: 7, of which 6 were waited for; matrix products, arithmetic and copies ran while one was open for 7% of the time, Pallas kernels for 0%

commit v1 on v0

--- a/solution.py
+++ b/solution.py
@@ -60,8 +60,13 @@
     )
     key_heads = key_vectors.reshape(tok_dev, local_heads, head_dim)
     value_heads = value_vectors.reshape(tok_dev, local_heads, head_dim)
-    key_part = lax.all_gather(key_heads, "sp", axis=0, tiled=True)
-    value_part = lax.all_gather(value_heads, "sp", axis=0, tiled=True)
+    key_part, value_part = jnp.split(
+        lax.all_gather(
+            jnp.concatenate([key_heads, value_heads], axis=1), axis_name="sp", axis=0, tiled=True
+        ),
+        [key_heads.shape[1]],
+        axis=1,
+    )
     part_rows = key_part.shape[0]
     block_size = math.gcd(part_rows, 512)
     key_blocks = key_part.reshape(part_rows // block_size, block_size, local_heads, head_dim)

time: 385 us -> 374 us (0.971)
  waiting for transfers between devices: 211 us -> 203 us
    all_gather x2 -> x1, waiting for transfers between devices: 40.3 us -> 33.3 us  [shards(): lax.all_gather(jnp.concatenate([key_heads, value_heads], axis=1), axis_na...]
    reshape x2 -> x0, local copies, waits for them, and re-layouts: 6.41 us -> none  [the longest x1 3.21 us: shards(): value_part.reshape(part_rows // block_size, block_size, local_heads, head...]
  transfers between devices with their start and end apart: 7 -> 6, of which waited for: 6 -> 5; matrix products, arithmetic and copies ran while one was open for 7% -> 6% of each run, Pallas kernels for 0% -> 0%
where the time goes in v1:
time: 374 us; the launch traced here: 373 us
  waiting for transfers between devices  203 us (54%)
  blocking collectives  72.1 us (19%)
  local copies, waits for them, and re-layouts  35 us (9%)
  matrix products  20.8 us (6%)
  other arithmetic  17.9 us (5%)
  between operations  13.5 us (4%)
  loops' own time  5.65 us (2%)
  starting transfers between devices  4.98 us (1%)
    all_gather x1, waiting for transfers between devices, shards(): lax.all_gather(lax.all_to_all(outgoing, 'sp', split_axis=0, concat_axis=0...  59 us
    all_gather x1, waiting for transfers between devices, shards(): lax.all_gather(attended, 'tp', axis=1, tiled=True)  54.2 us
    all_to_all x1, blocking collectives, shards(): lax.all_to_all(outgoing, 'sp', split_axis=0, concat_axis=0, tiled=True)  36.8 us
    all_gather x1, waiting for transfers between devices, shards(): lax.all_gather(jnp.concatenate([key_heads, value_heads], axis=1), axis_na...  33.3 us
    all_gather x1, waiting for transfers between devices, shards(): hidden_all = lax.all_gather(hidden, 'tp', axis=3, tiled=True)  28.1 us
    all_gather x1, waiting for transfers between devices, shards(): normed = lax.all_gather(normed_own, 'tp', axis=1, tiled=True)  27.9 us
    all_gather x1, blocking collectives, shards(): all_gates = lax.all_gather(log_gate_sums, 'sp', axis=0, tiled=True)  15.8 us
    all_gather x1, blocking collectives, shards(): lax.all_gather(shared_mid, 'tp', axis=1, tiled=True)  10.6 us
  transfers between devices with their start and end apart: 6, of which 5 were waited for; matrix products, arithmetic and copies ran while one was open for 6% of the time, Pallas kernels for 0%

profile of v1, /device:TPU:0, one launch (start us, length us, event | category | flops | bytes accessed | tf_op | source)
XLA Modules:
  0.0 373.1 jit_solution(18007078552913371516)
XLA Ops:
  6.6 1.2 copy.34
  7.8 1.1 copy.35
  8.9 0.8 pad_maximum_fusion
  9.8 0.0 all-gather.8.cloned.1.call-start
  9.9 0.1 copy.40
  10.0 0.2 eq.29
  10.2 0.2 eq.25
  10.4 0.1 copy.36
  10.5 15.8 %all_gather.22 = f32[4096,4]{0,1:T(4,128)S(1)} all-gather(f32[512,4]{0,1:T(4,128)S(1)} %copy-done.9), channel_id=1, replica_groups=mesh['sp'=8,'tp'=4] {'sp'}, dimensions={0}, use_global_device_ids=true | all-gather | bytes 73728 | tf_op jit(solution)/shard_map/all_gather | solution.py:55
  26.3 33.3 %all-gather.6.cloned.1.call-done = bf16[4096,8,64]{0,2,1:T(8,128)(2,1)} async-done(((bf16[512,8,64]{0,2,1:T(8,128)(2,1)}), bf16[4096,8,64]{0,2,1:T(8,128)(2,1)}) %all-gather.6.cloned.1.call-update) | async-done | bytes 4194320 | tf_op jit(solution)/shard_map/all_gather | solution.py:64
  59.6 2.7 fusion.62
  62.3 2.5 copy_bitcast_fusion
  64.9 16.6 %while.17 = (s32[]{:T(128)}, f32[4,512]{1,0:T(4,128)S(1)}, f32[4,512]{1,0:T(4,128)S(1)}, f32[4,512,64]{1,2,0:T(8,128)S(1)}, s32[8]{0:T(128)S(1)}, /*index=5*/s32...) while((s32[]{:T(128)}, f32[4,512]{1,0:T(4,128)S(1)}, ...), condition=%wide.region_5.6_spmd.clone, body=%wide.region_0.5_spmd.clone.sunk | while | flops 286790656 | bytes 15676785 | solution.py:107
  64.9 0.6 dynamic_slice.48
  66.2 6.3 %conditional.3 = ((f32[4,512]{1,0:T(4,128)S(1)}, f32[4,512]{1,0:T(4,128)S(1)}, f32[4,512,64]{1,2,0:T(8,128)S(1)})) conditional(s32[]{:T(128)} %convert_element_type.105, (f32[4,512]{1,0:T(4,128)S(1)}, f32[4,512]{1,0:T(4,128)S(1)}, f32[4,512,64]{1,2,0:T(8,128)S(1)}) %tuple.52, (s32[]{:T(128)}, s32[]{:T(128)}, bf16[8,512,4,64]{1,3,2,0:T(8,128)(2,1)}, ...), branch_computations={%region_1.1_spmd, %region_2.4_spmd} | conditional | flops 286790656 | bytes 15674446 | solution.py:104
  66.2 0.1 dynamic-slice_bitcast_fusion
  66.3 0.2 broadcast_compare_fusion
  66.5 2.2 fusion.2
  68.8 1.4 fusion.6
  70.1 2.3 fusion.10
  72.5 0.6 dynamic_slice.48
  73.8 0.6 dynamic_slice.48
  75.1 0.6 dynamic_slice.48
  76.4 0.6 dynamic_slice.48
  77.7 0.6 dynamic_slice.48
  78.9 0.6 dynamic_slice.48
  80.2 0.6 dynamic_slice.48
  81.5 0.7 divide_convert_fusion
  82.3 0.0 all-gather.12.cloned.1.call-start
  82.4 9.0 %reduce-window.6 = s32[32,8,128]{2,1,0:T(8,128)S(1)} reduce-window(s32[32,8,128]{2,1,0:T(8,128)S(1)} %fusion.56, s32[]{:T(128)} %constant.93.clone.1), window={size=1x1x128 pad=0_0x0_0x127_0}, to_apply=%region_8.9 | reduce-window | flops 4161536 | bytes 262148 | tf_op jit(solution)/shard_map/reduce-window
  91.4 0.1 slice.12
  91.5 0.1 copy.42
  91.6 0.1 copy.43
  91.7 0.2 copy.39
  91.9 0.2 mul.108
  92.1 0.1 broadcast_add_fusion.1
  92.3 4.3 %scatter_custom_fusion = s32[1280]{0:T(1024)S(1)} fusion(s32[1024]{0:T(1024)S(1)} %bitcast.125, s32[1024]{0:T(1024)S(1)} %add_select_fusion, s32[]{:T(128)} %constant.98.clone.1), kind=kCustom, calls=%fused_computation.76 | custom fusion | bytes 5124 | tf_op jit(solution)/shard_map/scatter | solution.py:146
  96.6 0.8 dynamic-slice_convert_fusion
  97.4 54.2 %all-gather.8.cloned.1.call-done = bf16[512,1024]{0,1:T(8,128)(2,1)} async-done(((bf16[512,256]{0,1:T(8,128)(2,1)}), bf16[512,1024]{0,1:T(8,128)(2,1)}) %all-gather.8.cloned.1.call-update) | async-done | bytes 1048592 | tf_op jit(solution)/shard_map/all_gather | solution.py:113
  151.6 2.5 fusion.50
  154.1 8.9 %psum.7 = f32[512]{0:T(512)S(1)} all-reduce(f32[512]{0:T(512)S(1)} %get-tuple-element.337), channel_id=1, replica_groups=mesh['sp'=8,'tp'=4] {'tp'}, use_global_device_ids=true, to_apply=%region_7.8 | all-reduce | flops 512 | bytes 4096 | tf_op jit(solution)/shard_map/psum | solution.py:120
  163.1 0.2 fusion.52
  163.3 4.7 %gather_fusion = bf16[1280,512]{1,0:T(8,128)(2,1)} fusion(bf16[513,512]{1,0:T(8,128)(2,1)S(1)} %concatenate.7, s32[2048]{0:T(1024)S(1)} %pad_clamp_fusion), kind=kCustom, calls=%fused_computation | custom fusion | bytes 2626560 | tf_op jit(solution)/shard_map/gather | solution.py:151
  168.1 36.8 %all_to_all.10 = bf16[8,4,40,512]{3,2,1,0:T(8,128)(2,1)S(1)} all-to-all(bf16[8,4,40,512]{3,2,1,0:T(8,128)(2,1)} %bitcast.116), channel_id=1, replica_groups=mesh['sp'=8,'tp'=4] {'sp'}, dimensions={0} | all-to-all | bytes 2621440 | tf_op jit(solution)/shard_map/all_to_all | solution.py:153
  204.8 1.2 copy.44
  206.1 0.2 all-gather.14.cloned.1.call-start
  206.3 59.0 %all-gather.12.cloned.1.call-done = bf16[8,4,40,2048]{3,2,0,1:T(8,128)(2,1)} async-done(((bf16[8,4,40,512]{3,2,0,1:T(8,128)(2,1)}), bf16[8,4,40,2048]{3,2,0,1:T(8,128)(2,1)}) %all-gather.12.cloned.1.call-update) | async-done | bytes 5242896 | tf_op jit(solution)/shard_map/all_gather | solution.py:152
  265.4 4.8 %fusion.37 = f32[8,4,40,128]{3,2,0,1:T(8,128)S(1)} fusion(bf16[8,4,40,2048]{3,2,0,1:T(8,128)(2,1)} %all-gather.12.cloned.1.call-done, bf16[4,2048,128]{2,1,0:T(8,128)(2,1)} %param.28), kind=kOutput, calls=%fused_computation.48 | convolution fusion | flops 671088640 | bytes 7995392 | tf_op jit(solution)/shard_map/secd,edf->secf/dot_general | solution.py:158
  270.2 0.5 copy-done.13
  270.7 2.3 fusion.46
  273.0 0.5 all-gather.10.cloned.1.call-update
  273.6 28.1 %all-gather.14.cloned.1.call-done = bf16[8,4,40,512]{3,2,0,1:T(8,128)(2,1)} async-done(((bf16[8,4,40,128]{3,2,0,1:T(8,128)(2,1)}), bf16[8,4,40,512]{3,2,0,1:T(8,128)(2,1)}) %all-gather.14.cloned.1.call-update) | async-done | bytes 1310736 | tf_op jit(solution)/shard_map/all_gather | solution.py:163
  301.7 2.2 fusion.31
  303.8 1.2 copy.45
  305.0 4.6 %all-to-all-start.1 = ((bf16[8,4,40,512]{3,2,1,0:T(8,128)(2,1)}), bf16[8,4,40,512]{3,2,1,0:T(8,128)(2,1)S(1)}, u32[]{:S(2)}, u32[]{:S(2)}) async-start(bf16[8,4,40,512]{3,2,1,0:T(8,128)(2,1)} %copy.45), calls=%async_computation.1 | async-start | bytes 2621440 | tf_op jit(solution)/shard_map/all_to_all | solution.py:167
  309.6 0.8 copy.46
  310.5 27.9 %all-gather.10.cloned.1.call-done = bf16[512,2048]{1,0:T(8,128)(2,1)} async-done(((bf16[512,512]{1,0:T(8,128)(2,1)}), bf16[512,2048]{1,0:T(8,128)(2,1)}) %all-gather.10.cloned.1.call-update) | async-done | bytes 2097168 | tf_op jit(solution)/shard_map/all_gather | solution.py:126
  338.4 2.5 fusion.63
  341.0 0.7 fusion.49
  341.7 10.6 %all_gather.25 = bf16[512,512]{1,0:T(8,128)(2,1)} all-gather(bf16[512,128]{1,0:T(8,128)(2,1)S(1)} %fusion.49), channel_id=1, replica_groups=mesh['sp'=8,'tp'=4] {'tp'}, dimensions={1}, use_global_device_ids=true | all-gather | bytes 655360 | tf_op jit(solution)/shard_map/all_gather | solution.py:133
  352.3 5.1 %gather_fusion.1 = bf16[1024,512]{1,0:T(8,128)(2,1)} fusion(bf16[1280,512]{1,0:T(8,128)(2,1)S(1)} %bitcast.113, s32[1024]{0:T(1024)S(1)} %broadcast_clamp_fusion), kind=kCustom, calls=%fused_computation.1 | custom fusion | bytes 2101248 | tf_op jit(solution)/shard_map/gather | solution.py:169
  357.4 3.4 reshape.124
  360.8 4.5 %multiply_reduce_fusion = f32[512,512]{1,0:T(8,128)S(1)} fusion(f32[512,2,512]{2,1,0:T(2,128)} %reshape.124, f32[512,2]{1,0:T(8,128)S(1)} %copy-done.7), kind=kLoop, calls=%fused_computation.38 | loop fusion | flops 786432 | bytes 3149824 | tf_op jit(solution)/shard_map/reduce_sum | solution.py:170
  365.3 1.2 fusion.36
  (71 shorter events, 0.5 us)
Async XLA Ops:
  6.5 295.1 %copy-start = (bf16[4,512,512]{2,1,0:T(8,128)(2,1)S(1)}, bf16[4,512,512]{2,1,0:T(8,128)(2,1)}, u32[]{:S(2)}) copy-start(bf16[4,512,512]{2,1,0:T(8,128)(2,1)} %param.30) | copy-start | bytes 6291460
  6.5 3.3 copy-start.11
  6.5 3.8 %copy-start.10 = (bf16[512,256]{1,0:T(8,128)(2,1)S(1)}, bf16[512,256]{1,0:T(8,128)(2,1)}, u32[]{:S(2)}) copy-start(bf16[512,256]{1,0:T(8,128)(2,1)} %param.19) | copy-start | bytes 786436
  6.5 4.0 %copy-start.9 = (f32[512,4]{0,1:T(4,128)S(1)}, f32[512,4]{0,1:T(4,128)}, u32[]{:S(2)}) copy-start(f32[512,4]{0,1:T(4,128)} %param.22) | copy-start | bytes 24580
  6.5 53.1 %all-gather.6.cloned.1.call-start = ((), (), s32[]{:S(2)}) async-start(), calls=%async_computation.2 | async-start | bytes 4718592 | tf_op jit(solution)/shard_map/all_gather | solution.py:64
  9.8 141.8 %all-gather.8.cloned.1.call-start = ((), (), s32[]{:S(2)}) async-start(), calls=%async_computation.3 | async-start | bytes 1310720 | tf_op jit(solution)/shard_map/all_gather | solution.py:113
  82.3 183.1 %all-gather.12.cloned.1.call-start = ((), (), s32[]{:S(2)}) async-start(), calls=%async_computation.5 | async-start | bytes 6553600 | tf_op jit(solution)/shard_map/all_gather | solution.py:152
  154.1 9.2 %copy-start.5 = (bf16[512,512]{1,0:T(8,128)(2,1)}, bf16[512,512]{1,0:T(8,128)(2,1)S(1)}, u32[]{:S(2)}) copy-start(bf16[512,512]{1,0:T(8,128)(2,1)S(1)} %get-tuple-element.338) | copy-start | bytes 1572868
  163.3 4.8 %copy-start.2 = (bf16[512,512]{1,0:T(8,128)(2,1)}, bf16[512,512]{1,0:T(8,128)(2,1)S(1)}, u32[]{:S(2)}) copy-start(bf16[512,512]{1,0:T(8,128)(2,1)S(1)} %fusion.52) | copy-start | bytes 1572868
  206.1 95.6 %all-gather.14.cloned.1.call-start = ((), (), s32[]{:S(2)}) async-start(), calls=%async_computation.6 | async-start | bytes 1638400 | tf_op jit(solution)/shard_map/all_gather | solution.py:163
  265.4 4.8 %copy-start.1 = (bf16[8,4,40,2048]{3,2,0,1:T(8,128)(2,1)S(1)}, bf16[8,4,40,2048]{3,2,0,1:T(8,128)(2,1)}, u32[]{:S(2)}) copy-start(bf16[8,4,40,2048]{3,2,0,1:T(8,128)(2,1)} %all-gather.12.cloned.1.call-done) | copy-start | bytes 15728644
  265.4 5.3 %copy-start.13 = (bf16[4,2048,128]{2,1,0:T(8,128)(2,1)S(1)}, bf16[4,2048,128]{2,1,0:T(8,128)(2,1)}, u32[]{:S(2)}) copy-start(bf16[4,2048,128]{2,1,0:T(8,128)(2,1)} %param.29) | copy-start | bytes 6291460
  273.0 65.4 %all-gather.10.cloned.1.call-start = ((), (), s32[]{:S(2)}) async-start(), calls=%async_computation.4 | async-start | bytes 2621440 | tf_op jit(solution)/shard_map/all_gather | solution.py:126
  303.8 5.8 %copy-start.12 = (f32[512,2]{0,1:T(2,128)S(1)}, f32[512,2]{0,1:T(2,128)}, u32[]{:S(2)}) copy-start(f32[512,2]{0,1:T(2,128)} %param.27) | copy-start | bytes 12292
  305.0 47.3 %all-to-all-start.1 = ((bf16[8,4,40,512]{3,2,1,0:T(8,128)(2,1)}), bf16[8,4,40,512]{3,2,1,0:T(8,128)(2,1)S(1)}, u32[]{:S(2)}, u32[]{:S(2)}) async-start(bf16[8,4,40,512]{3,2,1,0:T(8,128)(2,1)} %copy.45), calls=%async_computation.1 | async-start | bytes 2621440 | tf_op jit(solution)/shard_map/all_to_all | solution.py:167
  338.4 2.5 copy-start.3
  338.4 2.6 copy-start.14
  357.4 3.4 copy-start.7
  360.8 4.5 %copy-start.4 = (bf16[512,512]{1,0:T(8,128)(2,1)S(1)}, bf16[512,512]{1,0:T(8,128)(2,1)}, u32[]{:S(2)}) copy-start(bf16[512,512]{1,0:T(8,128)(2,1)} %all_gather.25) | copy-start | bytes 1572868
  360.8 4.5 %copy-start.6 = (bf16[512,512]{1,0:T(8,128)(2,1)S(1)}, bf16[512,512]{1,0:T(8,128)(2,1)}, u32[]{:S(2)}) copy-start(bf16[512,512]{1,0:T(8,128)(2,1)} %copy-done.5) | copy-start | bytes 1572868
  360.8 4.6 %copy-start.8 = (bf16[512,512]{1,0:T(8,128)(2,1)S(1)}, bf16[512,512]{1,0:T(8,128)(2,1)}, u32[]{:S(2)}) copy-start(bf16[512,512]{1,0:T(8,128)(2,1)} %param.33) | copy-start | bytes 1572868
Sparse Core Ops, SparseCore 0:
  9.9 49.6 all-gather.5
  82.4 69.1 all-gather.7
  206.2 59.1 all-gather.11
  273.1 28.5 all-gather.13
  303.3 35.0 all-gather.9
